TPU v7x, 32 devices: a whole 2x2x4 slice. The times are simulated.
32 devices in a mesh: gr: 2 (over core), sp: 8 (over z, y), tp: 2 (over x).
Axes of the slice: x: 2, y: 2, z: 4, core: 2. Of those that a mesh axis runs over, the one named last changes fastest.
Arguments:
- tokens: bfloat16 [4, 2048, 2048], P('gr', ('sp', 'tp')), parts along dimension 0, may hold values from -6 to 6
- key_weight: bfloat16 [2048, 1024], P('sp'), may hold values from -0.125 to 0.125
- value_weight: bfloat16 [2048, 1024], P('sp'), may hold values from -0.125 to 0.125
- queries: bfloat16 [4, 1024], P('gr'), parts along dimension 0, may hold values from -6 to 6
- head_offset: float32 [16], replicated, may hold values from -14 to -3.5
- key_bias: bfloat16 [4, 2048, 16], P('gr', ('sp', 'tp')), parts along dimension 0, may hold values from -0.5 to 12.9
Outputs:
- key_cache: bfloat16 [4, 2048, 1024], P('gr', 'sp', 'tp'), parts along dimension 0
- value_cache: bfloat16 [4, 2048, 1024], P('gr', 'sp', 'tp'), parts along dimension 0
- bias_cache: bfloat16 [4, 2048, 16], P('gr', 'sp', 'tp'), parts along dimension 0
- reading: float32 [4, 1024], P('gr', 'tp'), parts along dimension 0
There are 2 independent parts, one for each index of `gr`. A program takes and returns all parts, laid end to end along the dimension named above; an argument that names none is the same for every part. Nothing has to cross between parts.
All inputs are finite; a program needn't handle non-finite values.
Results may differ from a plain program's by a relative error of at most 0.0052.
Values may be sent and summed in bfloat16 or wider, within the bound.
A program may use at most 64 MiB of HBM per device.

v0:
```python
import jax
import jax.numpy as jnp
from jax import lax
from jax.sharding import PartitionSpec as P


def carried_in(x, axis, combine, identity):
    length, position = (lax.axis_size(axis), lax.axis_index(axis))
    everything = lax.all_gather(x, axis)
    start = jnp.broadcast_to(jnp.asarray(identity, x.dtype), x.shape)

    def lap(k, before):
        at = length - 1 - k
        reached = at > position
        new = combine(before, everything[at])
        return jnp.where(reached, new, before)

    return lax.fori_loop(0, length, lap, start)


def add_terms(earlier, later):
    return earlier + later


def normalize(mixture):
    return mixture * lax.rsqrt(jnp.mean(mixture * mixture, axis=-1, keepdims=True) + 1e-06)


def per_device(tokens, key_weight, value_weight, queries, head_offset, key_bias):
    seq_count, pos_dev, model_width = tokens.shape
    head_count = head_offset.shape[0]
    kv_width = key_weight.shape[1]
    head_dim = kv_width // head_count
    score_scale = head_dim ** (-0.5)
    tp_count = lax.axis_size("tp")
    col_width = kv_width // tp_count
    col_start = lax.axis_index("tp") * col_width
    own_cols = jnp.concatenate(
        [
            lax.dynamic_slice_in_dim(key_weight, col_start, col_width, 1),
            lax.dynamic_slice_in_dim(value_weight, col_start, col_width, 1),
        ],
        axis=1,
    )
    full_cols = lax.all_gather(own_cols, "sp", axis=0, tiled=True)
    projected = jnp.einsum(
        "spd,dw->spw",
        lax.all_gather(tokens, "tp", axis=1, tiled=True),
        full_cols,
        preferred_element_type=jnp.float32,
    ).astype(jnp.bfloat16)
    key_cache = projected[:, :, :col_width]
    value_cache = projected[:, :, col_width:]
    bias_cache = lax.all_to_all(key_bias, "tp", split_axis=2, concat_axis=1, tiled=True)
    span_len = key_cache.shape[1]
    local_heads = bias_cache.shape[2]
    key_blocks = key_cache.reshape(seq_count, span_len, local_heads, head_dim)
    value_blocks = value_cache.reshape(seq_count, span_len, local_heads, head_dim)
    query_cols = lax.dynamic_slice_in_dim(queries, col_start, col_width, 1)
    query_heads = query_cols.reshape(seq_count, local_heads, head_dim)
    head_start = lax.axis_index("tp") * local_heads
    local_offset = lax.dynamic_slice_in_dim(head_offset, head_start, local_heads, 0)
    logits = (
        jnp.einsum("sphc,shc->shp", key_blocks, query_heads, preferred_element_type=jnp.float32)
        * score_scale
    )
    logits = (
        logits
        + local_offset[None, :, None]
        + jnp.transpose(bias_cache.astype(jnp.float32), (0, 2, 1))
    )
    fading = jax.nn.log_sigmoid(-logits)
    within = lax.cumsum(fading, axis=2, reverse=True) - fading
    block_total = jnp.sum(fading, axis=2)
    carried = carried_in(block_total, "sp", add_terms, jnp.zeros_like(block_total))
    weights = jnp.exp(jax.nn.log_sigmoid(logits) + within + carried[:, :, None]).astype(
        jnp.bfloat16
    )
    partial_value = jnp.einsum(
        "shp,sphc->shc", weights, value_blocks, preferred_element_type=jnp.float32
    )
    mixture = lax.psum(partial_value, "sp")
    reading = normalize(mixture).reshape(seq_count, col_width)
    return (key_cache, value_cache, bias_cache, reading)


def solution(mesh):
    in_specs = (
        P("gr", ("sp", "tp"), None),
        P("sp", None),
        P("sp", None),
        P("gr", None),
        P(),
        P("gr", ("sp", "tp"), None),
    )
    out_specs = (P("gr", "sp", "tp"), P("gr", "sp", "tp"), P("gr", "sp", "tp"), P("gr", "tp"))
    return jax.shard_map(
        per_device, mesh=mesh, in_specs=in_specs, out_specs=out_specs, check_vma=False
    )
```

profile of v0, /device:TPU:0, one launch (start us, length us, event | category | flops | bytes accessed | tf_op | source)
XLA Modules:
  0.0 179.6 jit_solution(294673093222609058)
XLA Ops:
  7.2 0.0 copy-start
  7.2 0.0 all-gather.7.cloned.1.call-start
  7.2 0.7 all-gather.7.cloned.1.call-update
  7.9 0.0 all-gather.5.cloned.1.call-start
  8.0 1.1 constant_dynamic-slice_fusion.1
  9.1 0.1 copy.28
  9.2 0.1 copy.29
  9.3 0.8 pad_maximum_fusion
  10.2 0.0 all-gather.5.cloned.1.call-update
  10.2 0.6 copy.20
  10.8 4.2 %all-to-all-start = ((bf16[2,128,16]{1,0,2:T(2,128)(2,1)}), bf16[2,128,16]{1,0,2:T(2,128)(2,1)S(1)}, u32[]{:S(2)}, u32[]{:S(2)}) async-start(bf16[2,128,16]{1,0,2:T(2,128)(2,1)} %copy.20), calls=%async_computation | async-start | bytes 16384 | tf_op jit(solution)/shard_map/all_to_all | solution.py:54
  15.1 0.1 reshape.64
  15.1 0.1 dynamic_slice.25
  15.2 30.2 %all-gather.7.cloned.1.call-done = bf16[2,256,2048]{2,1,0:T(8,128)(2,1)} async-done(((bf16[2,128,2048]{2,1,0:T(8,128)(2,1)}), bf16[2,256,2048]{2,1,0:T(8,128)(2,1)}) %all-gather.7.cloned.1.call-update) | async-done | bytes 2097168 | tf_op jit(solution)/shard_map/all_gather | solution.py:48
  45.4 77.3 %all-gather.5.cloned.1.call-done = bf16[2048,1024]{0,1:T(8,128)(2,1)} async-done(((bf16[256,1024]{0,1:T(8,128)(2,1)}), bf16[2048,1024]{0,1:T(8,128)(2,1)}) %all-gather.5.cloned.1.call-update) | async-done | bytes 4194320 | tf_op jit(solution)/shard_map/all_gather | solution.py:45
  122.7 5.2 %fusion.5 = bf16[2,256,1024]{1,2,0:T(8,128)(2,1)S(1)} fusion(bf16[2,256,2048]{2,1,0:T(8,128)(2,1)} %all-gather.7.cloned.1.call-done, bf16[2048,1024]{0,1:T(8,128)(2,1)} %all-gather.5.cloned.1.call-done), kind=kOutput, calls=%fused_computation.4 | convolution fusion | flops 2148007936 | bytes 7340032 | tf_op jit(solution)/shard_map/spd,dw->spw/dot_general | solution.py:46
  127.9 0.1 fusion.18
  128.0 0.2 fusion.19
  128.2 1.0 copy.22
  129.2 0.1 negate_bitcast_fusion
  129.3 0.2 fusion.16
  129.5 17.7 %all-gather.1 = f32[8,2,8]{2,1,0:T(2,128)S(1)} all-gather(f32[1,2,8]{2,1,0:T(2,128)S(1)} %negate_bitcast_fusion.1), channel_id=2, replica_groups=mesh['gr'=2,'sp'=8,'tp'=2] {'sp'}, dimensions={0}, use_global_device_ids=true | all-gather | bytes 576 | tf_op jit(solution)/shard_map/all_gather | solution.py:9
  147.2 0.3 while.16
  147.5 5.0 %reduce-window.6 = f32[2,8,2,128]{3,1,2,0:T(8,128)S(1)} reduce-window(f32[2,8,2,128]{3,1,2,0:T(8,128)S(1)} %get-tuple-element.150, f32[]{:T(128)} %constant.72.clone.1), window={size=1x1x1x128 pad=0_0x0_0x0_0x0_127}, to_apply=%region_0.1 | reduce-window | flops 520192 | bytes 32772 | tf_op jit(solution)/shard_map/reduce-window
  152.5 0.1 slice_reduce_fusion
  152.6 1.0 copy.23
  153.6 0.1 fusion.17
  153.7 0.2 fusion.14
  153.9 17.9 %psum.7 = f32[2,8,64]{2,1,0:T(8,128)S(1)} all-reduce(f32[2,8,64]{2,1,0:T(8,128)S(1)} %bitcast.62), channel_id=1, replica_groups=mesh['gr'=2,'sp'=8,'tp'=2] {'sp'}, use_global_device_ids=true, to_apply=%region_5.6 | all-reduce | flops 1024 | bytes 8192 | tf_op jit(solution)/shard_map/psum | solution.py:82
  171.9 0.1 multiply_reduce_fusion
  172.0 0.1 broadcast_multiply_fusion
  172.1 0.7 reshape.53
  (22 shorter events, 0.2 us)
Async XLA Ops:
  7.2 7.9 %copy-start = (bf16[2,1024]{1,0:T(2,128)(2,1)S(1)}, bf16[2,1024]{1,0:T(2,128)(2,1)}, u32[]{:S(2)}) copy-start(bf16[2,1024]{1,0:T(2,128)(2,1)} %param.11) | copy-start | bytes 12292
  7.2 38.2 %all-gather.7.cloned.1.call-start = ((), (), s32[]{:S(2)}) async-start(), calls=%async_computation.2 | async-start | bytes 3145728 | tf_op jit(solution)/shard_map/all_gather | solution.py:48
  7.9 2.3 %copy-start.2 = (bf16[2,128,16]{1,2,0:T(8,128)(2,1)S(1)}, bf16[2,128,16]{1,2,0:T(8,128)(2,1)}, u32[]{:S(2)}) copy-start(bf16[2,128,16]{1,2,0:T(8,128)(2,1)} %param.13) | copy-start | bytes 24580
  7.9 7.2 %copy-start.3 = (f32[16]{0:T(128)S(1)}, f32[16]{0:T(128)}, u32[]{:S(2)}) copy-start(f32[16]{0:T(128)} %param.12) | copy-start | bytes 196
  7.9 114.7 %all-gather.5.cloned.1.call-start = ((), (), s32[]{:S(2)}) async-start(), calls=%async_computation.1 | async-start | bytes 4718592 | tf_op jit(solution)/shard_map/all_gather | solution.py:45
  10.8 118.4 %all-to-all-start = ((bf16[2,128,16]{1,0,2:T(2,128)(2,1)}), bf16[2,128,16]{1,0,2:T(2,128)(2,1)S(1)}, u32[]{:S(2)}, u32[]{:S(2)}) async-start(bf16[2,128,16]{1,0,2:T(2,128)(2,1)} %copy.20), calls=%async_computation | async-start | bytes 16384 | tf_op jit(solution)/shard_map/all_to_all | solution.py:54
  129.3 43.5 %copy-start.1 = (bf16[2,256,8]{1,2,0:T(8,128)(2,1)}, bf16[2,256,8]{1,2,0:T(8,128)(2,1)S(1)}, u32[]{:S(2)}) copy-start(bf16[2,256,8]{1,2,0:T(8,128)(2,1)S(1)} %get-tuple-element.151) | copy-start | bytes 24580
Sparse Core Ops, SparseCore 0:
  9.5 35.8 all-gather.6
  48.0 74.6 all-gather.4
where the time goes:
time: 180 us
  waiting for transfers between devices  108 us (60%)
  blocking collectives  35.7 us (20%)
  between operations  14.2 us (8%)
  other arithmetic  6.49 us (4%)
  matrix products  5.64 us (3%)
  local copies, waits for them, and re-layouts  4.99 us (3%)
  starting transfers between devices  4.31 us (2%)
    all_gather x1, waiting for transfers between devices, per_device(): full_cols = lax.all_gather(own_cols, 'sp', axis=0, tiled=True)  77.3 us
    all_gather x1, waiting for transfers between devices, per_device(): lax.all_gather(tokens, 'tp', axis=1, tiled=True)  30.2 us
    psum x1, blocking collectives, per_device(): mixture = lax.psum(partial_value, 'sp')  17.9 us
    all_gather x1, blocking collectives, carried_in(): everything = lax.all_gather(x, axis)  17.7 us
    dot_general x1, matrix products, per_device(): jnp.einsum('spd,dw->spw', lax.all_gather(tokens, 'tp', axis=1, tiled=True...  5.22 us
    another operation x2, other arithmetic  5.02 us
    all_to_all x1, starting transfers between devices, per_device(): lax.all_to_all(key_bias, 'tp', split_axis=2, concat_axis=1, tiled=True)  4.23 us
  transfers between devices with their start and end apart: 3, of which 2 were waited for; matrix products, arithmetic and copies ran while one was open for 5% of the time, Pallas kernels for 0%

commit v1 on v0

--- a/solution.py
+++ b/solution.py
@@ -2,6 +2,25 @@
 import jax.numpy as jnp
 from jax import lax
 from jax.sharding import PartitionSpec as P
+
+
+def joined_along(blocks, dim):
+    blocks = jnp.moveaxis(blocks, 0, dim)
+    dims = blocks.shape
+    return blocks.reshape(*dims[:dim], dims[dim] * dims[dim + 1], *dims[dim + 2 :])
+
+
+def on_each_block(x, axis, dim, work, out_dim):
+    devices, index, rows = (lax.axis_size(axis), lax.axis_index(axis), x.shape[dim])
+    forward = [(i, (i + 1) % devices) for i in range(devices)]
+    blocks = []
+    current = x
+    for turn in range(devices):
+        following = current if turn == devices - 1 else lax.ppermute(current, axis, forward)
+        blocks.append(work(current, (index - turn) % devices * rows))
+        current = following
+    blocks = jnp.stack(blocks)[(index - jnp.arange(devices)) % devices]
+    return joined_along(blocks, out_dim)
 
 
 def carried_in(x, axis, combine, identity):
@@ -43,11 +62,14 @@
         axis=1,
     )
     full_cols = lax.all_gather(own_cols, "sp", axis=0, tiled=True)
-    projected = jnp.einsum(
-        "spd,dw->spw",
-        lax.all_gather(tokens, "tp", axis=1, tiled=True),
-        full_cols,
-        preferred_element_type=jnp.float32,
+    projected = on_each_block(
+        tokens,
+        "tp",
+        1,
+        lambda own_block, offset: jnp.einsum(
+            "spd,dw->spw", own_block, full_cols, preferred_element_type=jnp.float32
+        ),
+        1,
     ).astype(jnp.bfloat16)
     key_cache = projected[:, :, :col_width]
     value_cache = projected[:, :, col_width:]

time: 180 us -> 145 us (0.81)
  waiting for transfers between devices: 108 us -> 70.1 us
  starting transfers between devices: 4.31 us -> 6.3 us
    all_gather x1 -> x0, waiting for transfers between devices: 30.2 us -> none  [per_device(): lax.all_gather(tokens, 'tp', axis=1, tiled=True)]
    all_gather x1, waiting for transfers between devices: 77.3 us -> 70.1 us  [per_device(): full_cols = lax.all_gather(own_cols, 'sp', axis=0, tiled=True)]
    ppermute x0 -> x1, starting transfers between devices: none -> 3.03 us  [on_each_block(): lax.ppermute(current, axis, forward)]
    another operation x2 -> x3, other arithmetic: 5.02 us -> 5.11 us
    dot_general x1 -> x2, matrix products: 5.22 us -> 5.27 us  [per_device(): jnp.einsum('spd,dw->spw', own_block, full_cols, preferred_element_type=jn...]
  transfers between devices with their start and end apart: 3 -> 3, of which waited for: 2 -> 1; matrix products, arithmetic and copies ran while one was open for 5% -> 6% of each run, Pallas kernels for 0% -> 0%
where the time goes in v1:
time: 145 us
  waiting for transfers between devices  70.1 us (48%)
  blocking collectives  35.7 us (25%)
  between operations  14.2 us (10%)
  other arithmetic  6.62 us (5%)
  starting transfers between devices  6.3 us (4%)
  local copies, waits for them, and re-layouts  6.05 us (4%)
  matrix products  5.69 us (4%)
    all_gather x1, waiting for transfers between devices, per_device(): full_cols = lax.all_gather(own_cols, 'sp', axis=0, tiled=True)  70.1 us
    psum x1, blocking collectives, per_device(): mixture = lax.psum(partial_value, 'sp')  17.9 us
    all_gather x1, blocking collectives, carried_in(): everything = lax.all_gather(x, axis)  17.7 us
    dot_general x2, matrix products, per_device(): jnp.einsum('spd,dw->spw', own_block, full_cols, preferred_element_type=jn...  5.27 us
    another operation x2, other arithmetic  5.02 us
    all_to_all x1, starting transfers between devices, per_device(): lax.all_to_all(key_bias, 'tp', split_axis=2, concat_axis=1, tiled=True)  3.23 us
    ppermute x1, starting transfers between devices, on_each_block(): lax.ppermute(current, axis, forward)  3.03 us
  transfers between devices with their start and end apart: 3, of which 1 were waited for; matrix products, arithmetic and copies ran while one was open for 6% of the time, Pallas kernels for 0%

profile of v1, /device:TPU:0, one launch (start us, length us, event | category | flops | bytes accessed | tf_op | source)
XLA Modules:
  0.0 144.9 jit_solution(106371043367519002)
XLA Ops:
  7.2 0.0 all-gather.4.cloned.1.call-start
  7.2 1.1 constant_dynamic-slice_fusion.1
  8.3 0.1 copy.28
  8.4 0.1 copy.29
  8.6 0.8 pad_maximum_fusion.1
  9.4 3.0 %collective-permute-start = (bf16[2,128,2048]{2,1,0:T(8,128)(2,1)}, bf16[2,128,2048]{2,1,0:T(8,128)(2,1)S(1)}, u32[]{:S(2)}, u32[]{:S(2)}) collective-permute-start(bf16[2,128,2048]{2,1,0:T(8,128)(2,1)} %param.8), channel_id=1, source_target_pairs={{0,1},{1,0},{2,3},{3,2},{4,5},{5,4},{6,7},{7,6},{8,9},{9,8},{10,11... | collective-permute-start | bytes 3145736 | tf_op jit(solution)/shard_map/ppermute | solution.py:19
  12.5 1.3 copy.20
  13.8 3.2 %all-to-all-start = ((bf16[2,128,16]{1,0,2:T(2,128)(2,1)}), bf16[2,128,16]{1,0,2:T(2,128)(2,1)S(1)}, u32[]{:S(2)}, u32[]{:S(2)}) async-start(bf16[2,128,16]{1,0,2:T(2,128)(2,1)} %copy.20), calls=%async_computation | async-start | bytes 16384 | tf_op jit(solution)/shard_map/all_to_all | solution.py:76
  17.0 0.1 reshape.123
  17.1 0.7 dynamic_slice.25
  17.9 70.1 %all-gather.4.cloned.1.call-done = bf16[2048,1024]{0,1:T(8,128)(2,1)} async-done(((bf16[256,1024]{0,1:T(8,128)(2,1)}), bf16[2048,1024]{0,1:T(8,128)(2,1)}) %all-gather.4.cloned.1.call-update) | async-done | bytes 4194320 | tf_op jit(solution)/shard_map/all_gather | solution.py:64
  88.0 3.9 %fusion.4 = bf16[1,2,128,1024]{2,3,1,0:T(8,128)(2,1)S(1)} fusion(bf16[2,128,2048]{2,1,0:T(8,128)(2,1)} %param.8, bf16[2048,1024]{0,1:T(8,128)(2,1)} %all-gather.4.cloned.1.call-done), kind=kOutput, calls=%fused_computation.7 | convolution fusion | flops 1073741824 | bytes 5767168 | tf_op jit(solution)/shard_map/spd,dw->spw/dot_general | solution.py:69
  92.0 1.4 fusion.7
  93.3 0.1 pad_maximum_fusion
  93.4 0.7 gather_fusion
  94.2 0.5 copy.19
  94.7 0.1 fusion.22
  94.8 0.2 copy.22
  95.0 0.2 fusion.23
  95.2 0.1 negate_bitcast_fusion
  95.3 0.2 fusion.18
  95.5 17.7 %all-gather.1 = f32[8,2,8]{2,1,0:T(2,128)S(1)} all-gather(f32[1,2,8]{2,1,0:T(2,128)S(1)} %negate_bitcast_fusion.1), channel_id=2, replica_groups=mesh['gr'=2,'sp'=8,'tp'=2] {'sp'}, dimensions={0}, use_global_device_ids=true | all-gather | bytes 576 | tf_op jit(solution)/shard_map/all_gather | solution.py:28
  113.3 0.3 while.16
  113.6 5.0 %reduce-window.6 = f32[2,8,2,128]{3,1,2,0:T(8,128)S(1)} reduce-window(f32[2,8,2,128]{3,1,2,0:T(8,128)S(1)} %get-tuple-element.138, f32[]{:T(128)} %constant.88.clone.1), window={size=1x1x1x128 pad=0_0x0_0x0_0x0_127}, to_apply=%region_0.1 | reduce-window | flops 520192 | bytes 32772 | tf_op jit(solution)/shard_map/reduce-window
  118.5 0.1 slice_reduce_fusion
  118.7 0.2 copy.23
  118.9 0.1 fusion.19
  119.0 0.2 fusion.16
  119.2 17.9 %psum.7 = f32[2,8,64]{2,1,0:T(8,128)S(1)} all-reduce(f32[2,8,64]{2,1,0:T(8,128)S(1)} %bitcast.79), channel_id=1, replica_groups=mesh['gr'=2,'sp'=8,'tp'=2] {'sp'}, use_global_device_ids=true, to_apply=%region_5.6 | all-reduce | flops 1024 | bytes 8192 | tf_op jit(solution)/shard_map/psum | solution.py:104
  137.2 0.1 multiply_reduce_fusion
  137.3 0.1 broadcast_multiply_fusion
  137.3 0.7 reshape.104
  (29 shorter events, 0.3 us)
Async XLA Ops:
  7.2 9.9 %copy-start = (bf16[2,1024]{1,0:T(2,128)(2,1)S(1)}, bf16[2,1024]{1,0:T(2,128)(2,1)}, u32[]{:S(2)}) copy-start(bf16[2,1024]{1,0:T(2,128)(2,1)} %param.11) | copy-start | bytes 12292
  7.2 80.8 %all-gather.4.cloned.1.call-start = ((), (), s32[]{:S(2)}) async-start(), calls=%async_computation.1 | async-start | bytes 4718592 | tf_op jit(solution)/shard_map/all_gather | solution.py:64
  9.4 82.5 %collective-permute-start = (bf16[2,128,2048]{2,1,0:T(8,128)(2,1)}, bf16[2,128,2048]{2,1,0:T(8,128)(2,1)S(1)}, u32[]{:S(2)}, u32[]{:S(2)}) collective-permute-start(bf16[2,128,2048]{2,1,0:T(8,128)(2,1)} %param.8), channel_id=1, source_target_pairs={{0,1},{1,0},{2,3},{3,2},{4,5},{5,4},{6,7},{7,6},{8,9},{9,8},{10,11... | collective-permute-start | bytes 3145736 | tf_op jit(solution)/shard_map/ppermute | solution.py:19
  13.8 81.5 %all-to-all-start = ((bf16[2,128,16]{1,0,2:T(2,128)(2,1)}), bf16[2,128,16]{1,0,2:T(2,128)(2,1)S(1)}, u32[]{:S(2)}, u32[]{:S(2)}) async-start(bf16[2,128,16]{1,0,2:T(2,128)(2,1)} %copy.20), calls=%async_computation | async-start | bytes 16384 | tf_op jit(solution)/shard_map/all_to_all | solution.py:76
  88.0 3.9 %copy-start.4 = (bf16[2048,1024]{0,1:T(8,128)(2,1)S(1)}, bf16[2048,1024]{0,1:T(8,128)(2,1)}, u32[]{:S(2)}) copy-start(bf16[2048,1024]{0,1:T(8,128)(2,1)} %all-gather.4.cloned.1.call-done) | copy-start | bytes 12582916
  94.8 43.2 %copy-start.1 = (bf16[2,256,512]{2,1,0:T(8,128)(2,1)}, bf16[2,256,512]{2,1,0:T(8,128)(2,1)S(1)}, u32[]{:S(2)}) copy-start(bf16[2,256,512]{2,1,0:T(8,128)(2,1)S(1)} %get-tuple-element.140) | copy-start | bytes 1572868
  94.8 43.2 %copy-start.2 = (bf16[2,256,512]{2,1,0:T(8,128)(2,1)}, bf16[2,256,512]{2,1,0:T(8,128)(2,1)S(1)}, u32[]{:S(2)}) copy-start(bf16[2,256,512]{2,1,0:T(8,128)(2,1)S(1)} %get-tuple-element.141) | copy-start | bytes 1572868
  95.3 42.7 %copy-start.3 = (bf16[2,256,8]{1,2,0:T(8,128)(2,1)}, bf16[2,256,8]{1,2,0:T(8,128)(2,1)S(1)}, u32[]{:S(2)}) copy-start(bf16[2,256,8]{1,2,0:T(8,128)(2,1)S(1)} %get-tuple-element.139) | copy-start | bytes 24580
Sparse Core Ops, SparseCore 0:
  10.6 77.3 all-gather.3
